TPU v7x, 32 devices: a whole 2x2x4 slice. The times are simulated.
32 devices in a mesh: sp: 4 (over x, core), dp: 8 (over z, y).
Axes of the slice: x: 2, y: 2, z: 4, core: 2. Of those that a mesh axis runs over, the one named last changes fastest.
Arguments:
- query: bfloat16 [8, 512, 1024], P('dp', None, 'sp'), may hold values from -120 to 120
- keys: bfloat16 [8, 512, 1024], P('dp', None, 'sp'), may hold values from -6 to 6
- values: bfloat16 [8, 512, 1024], P('dp', None, 'sp'), may hold values from -6 to 6
- output: bfloat16 [8, 512, 1024], P('dp'), may hold values from -1 to 1
- cum: float32 [8, 16, 512], P('dp', 'sp'), as said below
- d_out: bfloat16 [8, 512, 2048], P('dp', 'sp'), may hold values from -6 to 6
- w_out: bfloat16 [1024, 2048], P('dp'), may hold values from -0.125 to 0.125
Outputs:
- d_query: bfloat16 [8, 512, 1024], P('dp', 'sp')
- d_key: bfloat16 [8, 512, 1024], P('dp', 'sp')
- d_value: bfloat16 [8, 512, 1024], P('dp', 'sp')
- d_cum: float32 [8, 16, 512], P('dp', 'sp')
- d_w_out: float32 [1024, 2048], P('dp', 'sp')
Inputs may be any that keep to these rules, and one draw needn't show every extreme that they name: cum never rises along positions.
All inputs are finite; a program needn't handle non-finite values.
Results may differ from a plain program's by a relative error of at most 0.008.
Values may be sent and summed in bfloat16 or wider, within the bound.
A program may use at most 64 MiB of HBM per device.

v0:
```python
import jax
import jax.numpy as jnp
from jax import lax
from jax.sharding import PartitionSpec as P


def head_grads(query, keys, values, output, cotangent, cum):
    head_count, length, head_width = query.shape
    span_rows = min(512, length)
    score_scale = head_width ** (-0.5)
    row_dots = jnp.sum(cotangent.astype(jnp.float32) * output.astype(jnp.float32), axis=2)
    positions = jnp.arange(length)

    def product(left, right, form):
        return jnp.einsum(form, left, right, preferred_element_type=jnp.float32)

    def advance(totals, block_index):
        key_grad, value_grad, cum_grad = totals
        offset = block_index * span_rows
        query_blk = lax.dynamic_slice_in_dim(query, offset, span_rows, 1)
        cot_blk = lax.dynamic_slice_in_dim(cotangent, offset, span_rows, 1)
        cum_blk = lax.dynamic_slice_in_dim(cum, offset, span_rows, 1)
        dots_blk = lax.dynamic_slice_in_dim(row_dots, offset, span_rows, 1)
        scores = product(query_blk, keys, "hqe,hke->hqk") * score_scale
        scores = scores + cum_blk[:, :, None] - cum[:, None, :]
        query_pos = offset + jnp.arange(span_rows)
        causal = positions[None, :] <= query_pos[:, None]
        scores = jnp.where(causal[None], scores, -1e30)
        row_max = jnp.max(scores, axis=2, keepdims=True)
        weights = jnp.exp(scores - row_max)
        weights = weights / jnp.sum(weights, axis=2, keepdims=True)
        weights_b = weights.astype(jnp.bfloat16)
        d_prob = product(cot_blk, values, "hqe,hke->hqk")
        d_score = weights * (d_prob - dots_blk[:, :, None])
        score_b = d_score.astype(jnp.bfloat16)
        query_grad = (product(score_b, keys, "hqk,hke->hqe") * score_scale).astype(jnp.bfloat16)
        key_grad = key_grad + product(score_b, query_blk, "hqk,hqe->hke") * score_scale
        value_grad = value_grad + product(weights_b, cot_blk, "hqk,hqe->hke")
        cum_grad = cum_grad - jnp.sum(d_score, axis=1)
        own_part = lax.dynamic_slice_in_dim(cum_grad, offset, span_rows, 1) + jnp.sum(
            d_score, axis=2
        )
        cum_grad = lax.dynamic_update_slice_in_dim(cum_grad, own_part, offset, 1)
        return ((key_grad, value_grad, cum_grad), query_grad)

    start_state = (
        jnp.zeros(query.shape, jnp.float32),
        jnp.zeros(query.shape, jnp.float32),
        jnp.zeros(cum.shape, jnp.float32),
    )
    totals, query_blocks = lax.scan(advance, start_state, jnp.arange(length // span_rows))
    query_grad = jnp.transpose(query_blocks, (1, 0, 2, 3)).reshape(query.shape)
    return (query_grad, totals[0].astype(jnp.bfloat16), totals[1].astype(jnp.bfloat16), totals[2])


def shards(query, keys, values, output, cum, d_out, w_out):
    local_rows = d_out[0]
    whole_output = output[0]
    d_attn = lax.dot_general(
        local_rows,
        lax.all_gather(w_out, "dp", axis=0, tiled=True),
        (((1,), (1,)), ((), ())),
        preferred_element_type=jnp.float32,
    ).astype(jnp.bfloat16)
    head_cot, column_part = (
        lax.all_to_all(d_attn[None], "sp", split_axis=2, concat_axis=1, tiled=True),
        lax.all_to_all(d_out, "sp", split_axis=2, concat_axis=1, tiled=True),
    )
    grad_weight = lax.psum_scatter(
        lax.dot_general(
            whole_output,
            column_part[0],
            (((0,), (0,)), ((), ())),
            preferred_element_type=jnp.float32,
        ),
        "dp",
        scatter_dimension=0,
        tiled=True,
    )
    head_cols = query.shape[2]
    head_count = cum.shape[1]
    head_width = head_cols // head_count
    seq_length = query.shape[1]
    own_output = lax.dynamic_slice_in_dim(
        whole_output, lax.axis_index("sp") * head_cols, head_cols, 1
    )

    def heads_first(matrix):
        return jnp.transpose(matrix.reshape(seq_length, head_count, head_width), (1, 0, 2))

    def tokens_first(matrix):
        return jnp.transpose(matrix, (1, 0, 2)).reshape(1, seq_length, head_cols)

    grads = head_grads(
        heads_first(query[0]),
        heads_first(keys[0]),
        heads_first(values[0]),
        heads_first(own_output),
        heads_first(head_cot[0]),
        cum[0],
    )
    query_grad, key_grad, value_grad = (
        lax.all_to_all(tokens_first(grads[0]), "sp", split_axis=1, concat_axis=2, tiled=True),
        lax.all_to_all(tokens_first(grads[1]), "sp", split_axis=1, concat_axis=2, tiled=True),
        lax.all_to_all(tokens_first(grads[2]), "sp", split_axis=1, concat_axis=2, tiled=True),
    )
    return (query_grad, key_grad, value_grad, grads[3][None], grad_weight)


def solution(mesh):
    placed = (
        P("dp", None, "sp"),
        P("dp", None, "sp"),
        P("dp", None, "sp"),
        P("dp", None, None),
        P("dp", "sp", None),
        P("dp", "sp", None),
        P("dp", None),
    )
    return jax.shard_map(
        shards,
        mesh=mesh,
        in_specs=placed,
        out_specs=(
            P("dp", "sp", None),
            P("dp", "sp", None),
            P("dp", "sp", None),
            P("dp", "sp", None),
            P("dp", "sp"),
        ),
        check_vma=False,
    )
```

profile of v0, /device:TPU:1, one launch (start us, length us, event | category | flops | bytes accessed | tf_op | source)
XLA Modules:
  0.0 161.3 jit_solution(12182984740562545491)
XLA Ops:
  7.9 2.4 %copy.99 = bf16[1,128,2048]{1,0,2:T(2,128)(2,1)S(1)} copy(bf16[1,128,2048]{2,1,0:T(8,128)(2,1)} %param.12) | data formatting | bytes 1048576 | tf_op args[5]
  10.8 11.5 %reduce.4 = bf16[2048,128]{1,0:T(8,128)(2,1)S(1)} reduce(bf16[2048,1,128]{2,1,0:T(2,128)(2,1)S(1)} %bitcast.83, bf16[]{:T(256)} %broadcast.48), dimensions={1}, to_apply=%bitcast.67.reduce_sub_computation | reduce | bytes 1048578
  22.5 12.2 %all_to_all.84 = bf16[4,2,32768]{2,1,0:T(2,128)(2,1)S(1)} all-to-all(bf16[4,2,32768]{2,1,0:T(2,128)(2,1)S(1)} %reshape.79), channel_id=1, replica_groups=mesh['sp'=4,'dp'=8] {'sp'}, dimensions={0} | all-to-all | bytes 1048576 | tf_op jit(solution)/shard_map/all_to_all | solution.py:67
  35.6 2.1 %fusion.15 = f32[1024,512]{1,0:T(8,128)} fusion(bf16[512,512]{1,0:T(8,128)(2,1)S(1)} %bitcast.85, bf16[1,512,1024]{2,1,0:T(8,128)(2,1)S(1)} %copy-done.1), kind=kOutput, calls=%fused_computation.20 | convolution fusion | flops 536870912 | bytes 3670016 | tf_op jit(solution)/shard_map/dot_general | solution.py:70
  39.2 44.6 %all-gather.2.cloned.1.call-done = bf16[1024,2048]{1,0:T(8,128)(2,1)} async-done(((bf16[128,2048]{1,0:T(8,128)(2,1)}), bf16[1024,2048]{1,0:T(8,128)(2,1)}) %all-gather.2.cloned.1.call-update) | async-done | bytes 4194320 | tf_op jit(solution)/shard_map/all_gather | solution.py:61
  83.8 3.7 %fusion.14 = bf16[1,128,1024]{2,1,0:T(8,128)(2,1)S(1)} fusion(bf16[1024,2048]{1,0:T(8,128)(2,1)} %all-gather.2.cloned.1.call-done, bf16[1,128,2048]{2,1,0:T(8,128)(2,1)S(1)} %copy-done), kind=kOutput, calls=%fused_computation.19 | convolution fusion | flops 537001984 | bytes 4980736 | tf_op jit(solution)/shard_map/dot_general | solution.py:59
  87.9 2.2 %reduce = bf16[1024,128]{1,0:T(8,128)(2,1)S(1)} reduce(bf16[1024,1,128]{2,1,0:T(2,128)(2,1)S(1)} %bitcast.92, bf16[]{:T(256)} %broadcast.48), dimensions={1}, to_apply=%bitcast.59.reduce_sub_computation | reduce | bytes 524290
  90.9 5.3 %all-to-all-start = ((bf16[4,2,16384]{2,1,0:T(2,128)(2,1)}), bf16[4,2,16384]{2,1,0:T(2,128)(2,1)S(1)}, u32[]{:S(2)}, u32[]{:S(2)}) async-start(bf16[4,2,16384]{2,1,0:T(2,128)(2,1)} %reshape.71), calls=%async_computation | async-start | bytes 524288 | tf_op jit(solution)/shard_map/all_to_all | solution.py:66
  96.2 3.4 %fusion.32 = (f32[4,512]{1,0:T(4,128)S(1)}, f32[4,512,512]{1,2,0:T(8,128)}) fusion(f32[4,512]{1,0:T(4,128)S(1)} %bitcast.112, pred[512,512]{0,1:T(8,128)(4,1)S(1)} %iota_compare_fusion, bf16[4,512,64]{1,2,0:T(8,128)(2,1)S(1)} %bitcast.97, bf16[4,512,64]{1,2,0:T(8,128)(2,1)S(1)} %bitcast.100), kind=kOutput, calls=%fused_computation.38 | convolution fusion | flops 140509696 | bytes 4997120 | tf_op jit(solution)/shard_map/while/body/eval_jaxpr/sub | solution.py:30
  99.6 1.6 %all-to-all-done = bf16[4,2,16384]{2,1,0:T(2,128)(2,1)S(1)} async-done(((bf16[4,2,16384]{2,1,0:T(2,128)(2,1)}), bf16[4,2,16384]{2,1,0:T(2,128)(2,1)S(1)}, u32[]{:S(2)}, u32[]{:S(2)}) %all-to-all-start) | async-done | bytes 262176 | tf_op jit(solution)/shard_map/all_to_all | solution.py:66
  102.0 3.5 %fusion.31 = (f32[4,512]{1,0:T(4,128)S(1)}, f32[4,512]{1,0:T(4,128)S(1)}, bf16[4,512,512]{1,2,0:T(8,128)(2,1)S(1)}) fusion(f32[4,512]{1,0:T(4,128)S(1)} %multiply_reduce_fusion, bf16[4,512,64]{1,2,0:T(8,128)(2,1)} %bitcast.111, bf16[512,4,64]{0,2,1:T(8,128)(2,1)S(1)} %reshape_squeeze.14, f32[4,512,512]{1,2,0:T(8,128)} %get-tuple-element.52, ...), kind=kOutput, calls=%fused_computation.37 | convolution fusion | flops 140505088 | bytes 6848512 | tf_op jit(solution)/shard_map/while/body/eval_jaxpr/hqe,hke->hqk/dot_general | solution.py:15
  106.7 3.0 %reduce.2 = bf16[512,256]{1,0:T(8,128)(2,1)} reduce(bf16[512,1,256]{2,1,0:T(2,128)(2,1)S(1)} %bitcast.93, bf16[]{:T(256)} %broadcast.48), dimensions={1}, to_apply=%bitcast.63.reduce_sub_computation | reduce | bytes 524290
  109.6 1.7 %reshape.75 = bf16[4,2,16384]{2,1,0:T(2,128)(2,1)} reshape(bf16[512,256]{1,0:T(8,128)(2,1)} %reduce.2) | data formatting | bytes 524288
  111.3 4.3 %all-to-all-start.2 = ((bf16[4,2,16384]{2,1,0:T(2,128)(2,1)}), bf16[4,2,16384]{2,1,0:T(2,128)(2,1)S(1)}, u32[]{:S(2)}, u32[]{:S(2)}) async-start(bf16[4,2,16384]{2,1,0:T(2,128)(2,1)} %reshape.75), calls=%async_computation.2 | async-start | bytes 524288 | tf_op jit(solution)/shard_map/all_to_all | solution.py:104
  116.6 2.2 %reduce.1 = bf16[512,256]{1,0:T(8,128)(2,1)S(1)} reduce(bf16[512,1,256]{2,1,0:T(2,128)(2,1)S(1)} %bitcast.94, bf16[]{:T(256)} %broadcast.48), dimensions={1}, to_apply=%bitcast.61.reduce_sub_computation | reduce | bytes 524290
  119.6 1.2 all-to-all-done.2
  120.7 4.3 %all-to-all-start.1 = ((bf16[4,2,16384]{2,1,0:T(2,128)(2,1)}), bf16[4,2,16384]{2,1,0:T(2,128)(2,1)S(1)}, u32[]{:S(2)}, u32[]{:S(2)}) async-start(bf16[4,2,16384]{2,1,0:T(2,128)(2,1)} %reshape.73), calls=%async_computation.1 | async-start | bytes 524288 | tf_op jit(solution)/shard_map/all_to_all | solution.py:103
  125.1 3.2 %fusion.11 = bf16[4,512,64]{1,2,0:T(8,128)(2,1)S(1)} fusion(f32[4,512]{1,0:T(4,128)S(1)} %get-tuple-element.38, bf16[512,4,64]{0,2,1:T(8,128)(2,1)S(1)} %copy-done.3, f32[4,512]{1,0:T(4,128)S(1)} %bitcast.113, pred[512,512]{0,1:T(8,128)(4,1)} %copy-done.7, bf16[4,512,64]{1,2,0:T(8,128)(2,1)S(1)} %bitcast.99, bf16[4,512,64]{1,2,0:T(8,128)(2,1)S(1)} %bitcast.102), kind=kOutput, calls=%fused_computation.18 | convolution fusion | flops 275909120 | bytes 1327104 | tf_op jit(solution)/shard_map/while/body/eval_jaxpr/hqk,hqe->hke/dot_general | solution.py:15
  128.7 2.2 %reduce.3 = bf16[512,256]{1,0:T(8,128)(2,1)S(1)} reduce(bf16[512,1,256]{2,1,0:T(2,128)(2,1)S(1)} %bitcast.91, bf16[]{:T(256)} %broadcast.48), dimensions={1}, to_apply=%bitcast.65.reduce_sub_computation | reduce | bytes 524290
  131.7 3.4 %all-to-all-start.3 = ((bf16[4,2,16384]{2,1,0:T(2,128)(2,1)}), bf16[4,2,16384]{2,1,0:T(2,128)(2,1)S(1)}, u32[]{:S(2)}, u32[]{:S(2)}) async-start(bf16[4,2,16384]{2,1,0:T(2,128)(2,1)} %reshape.77), calls=%async_computation.3 | async-start | bytes 524288 | tf_op jit(solution)/shard_map/all_to_all | solution.py:105
  136.2 0.9 copy.102
  137.6 0.9 copy.101
  138.4 1.7 %all-to-all-done.3 = bf16[4,2,16384]{2,1,0:T(2,128)(2,1)S(1)} async-done(((bf16[4,2,16384]{2,1,0:T(2,128)(2,1)}), bf16[4,2,16384]{2,1,0:T(2,128)(2,1)S(1)}, u32[]{:S(2)}, u32[]{:S(2)}) %all-to-all-start.3) | async-done | bytes 262176 | tf_op jit(solution)/shard_map/all_to_all | solution.py:105
  141.5 12.9 %reduce-scatter.2.cloned.1.call-done = f32[128,512]{1,0:T(8,128)} async-done(((f32[1024,512]{1,0:T(8,128)}), f32[128,512]{1,0:T(8,128)}) %reduce-scatter.2.cloned.1.call-update) | async-done | bytes 262160 | tf_op jit(solution)/shard_map/reduce_scatter | solution.py:69
  (59 shorter events, 12.5 us)
Async XLA Ops:
  7.2 76.6 %all-gather.2.cloned.1.call-start = ((), (), s32[]{:S(2)}) async-start(), calls=%async_computation.6 | async-start | bytes 4718592 | tf_op jit(solution)/shard_map/all_gather | solution.py:61
  7.9 146.6 %reduce-scatter.2.cloned.1.call-start = ((), (), s32[]{:S(2)}) async-start(), calls=%async_computation.7 | async-start | bytes 2359296 | tf_op jit(solution)/shard_map/reduce_scatter | solution.py:69
  10.3 25.3 %copy-start.1 = (bf16[1,512,1024]{2,1,0:T(8,128)(2,1)S(1)}, bf16[1,512,1024]{2,1,0:T(8,128)(2,1)}, u32[]{:S(2)}) copy-start(bf16[1,512,1024]{2,1,0:T(8,128)(2,1)} %param.10) | copy-start | bytes 3145732
  35.3 2.6 %copy-start.4 = (bf16[1,512,256]{2,1,0:T(8,128)(2,1)S(1)}, bf16[1,512,256]{2,1,0:T(8,128)(2,1)}, u32[]{:S(2)}) copy-start(bf16[1,512,256]{2,1,0:T(8,128)(2,1)} %param.7) | copy-start | bytes 786436
  35.6 2.6 %copy-start.5 = (bf16[1,512,256]{2,1,0:T(8,128)(2,1)S(1)}, bf16[1,512,256]{2,1,0:T(8,128)(2,1)}, u32[]{:S(2)}) copy-start(bf16[1,512,256]{2,1,0:T(8,128)(2,1)} %param.8) | copy-start | bytes 786436
  35.6 2.7 %copy-start.6 = (bf16[1,512,256]{2,1,0:T(8,128)(2,1)S(1)}, bf16[1,512,256]{2,1,0:T(8,128)(2,1)}, u32[]{:S(2)}) copy-start(bf16[1,512,256]{2,1,0:T(8,128)(2,1)} %param.9) | copy-start | bytes 786436
  35.6 48.2 %copy-start = (bf16[1,128,2048]{2,1,0:T(8,128)(2,1)S(1)}, bf16[1,128,2048]{2,1,0:T(8,128)(2,1)}, u32[]{:S(2)}) copy-start(bf16[1,128,2048]{2,1,0:T(8,128)(2,1)} %param.12) | copy-start | bytes 1572868
  38.3 57.9 %copy-start.8 = (f32[1,4,512]{2,1,0:T(4,128)S(1)}, f32[1,4,512]{2,1,0:T(4,128)}, u32[]{:S(2)}) copy-start(f32[1,4,512]{2,1,0:T(4,128)} %param.11) | copy-start | bytes 24580
  39.2 60.4 %copy-start.7 = (pred[512,512]{0,1:T(8,128)(4,1)}, pred[512,512]{0,1:T(8,128)(4,1)S(1)}, u32[]{:S(2)}) copy-start(pred[512,512]{0,1:T(8,128)(4,1)S(1)} %iota_compare_fusion) | copy-start | bytes 786436
  90.9 10.3 %all-to-all-start = ((bf16[4,2,16384]{2,1,0:T(2,128)(2,1)}), bf16[4,2,16384]{2,1,0:T(2,128)(2,1)S(1)}, u32[]{:S(2)}, u32[]{:S(2)}) async-start(bf16[4,2,16384]{2,1,0:T(2,128)(2,1)} %reshape.71), calls=%async_computation | async-start | bytes 524288 | tf_op jit(solution)/shard_map/all_to_all | solution.py:66
  101.9 3.6 %copy-start.2 = (bf16[512,4,64]{0,2,1:T(8,128)(2,1)}, bf16[512,4,64]{0,2,1:T(8,128)(2,1)S(1)}, u32[]{:S(2)}) copy-start(bf16[512,4,64]{0,2,1:T(8,128)(2,1)S(1)} %reshape_squeeze.14) | copy-start | bytes 786436
  106.7 18.4 %copy-start.3 = (bf16[512,4,64]{0,2,1:T(8,128)(2,1)S(1)}, bf16[512,4,64]{0,2,1:T(8,128)(2,1)}, u32[]{:S(2)}) copy-start(bf16[512,4,64]{0,2,1:T(8,128)(2,1)} %copy-done.2) | copy-start | bytes 786436
  111.3 9.4 %all-to-all-start.2 = ((bf16[4,2,16384]{2,1,0:T(2,128)(2,1)}), bf16[4,2,16384]{2,1,0:T(2,128)(2,1)S(1)}, u32[]{:S(2)}, u32[]{:S(2)}) async-start(bf16[4,2,16384]{2,1,0:T(2,128)(2,1)} %reshape.75), calls=%async_computation.2 | async-start | bytes 524288 | tf_op jit(solution)/shard_map/all_to_all | solution.py:104
  120.7 11.0 %all-to-all-start.1 = ((bf16[4,2,16384]{2,1,0:T(2,128)(2,1)}), bf16[4,2,16384]{2,1,0:T(2,128)(2,1)S(1)}, u32[]{:S(2)}, u32[]{:S(2)}) async-start(bf16[4,2,16384]{2,1,0:T(2,128)(2,1)} %reshape.73), calls=%async_computation.1 | async-start | bytes 524288 | tf_op jit(solution)/shard_map/all_to_all | solution.py:103
  131.7 8.5 %all-to-all-start.3 = ((bf16[4,2,16384]{2,1,0:T(2,128)(2,1)}), bf16[4,2,16384]{2,1,0:T(2,128)(2,1)S(1)}, u32[]{:S(2)}, u32[]{:S(2)}) async-start(bf16[4,2,16384]{2,1,0:T(2,128)(2,1)} %reshape.77), calls=%async_computation.3 | async-start | bytes 524288 | tf_op jit(solution)/shard_map/all_to_all | solution.py:105
Sparse Core Ops, SparseCore 0:
  10.1 73.6 all-gather.1
  87.9 66.5 reduce-scatter.1
where the time goes:
time: 164 us; the launch traced here: 161 us
  waiting for transfers between devices  62.7 us (38%)
  other arithmetic  21.9 us (13%)
  starting transfers between devices  17.4 us (11%)
  matrix products  17.1 us (10%)
  local copies, waits for them, and re-layouts  15.4 us (9%)
  between operations  14.4 us (9%)
  blocking collectives  12.2 us (7%)
    all_gather x1, waiting for transfers between devices, shards(): lax.all_gather(w_out, 'dp', axis=0, tiled=True)  44.6 us
    unnamed x5, other arithmetic  21.1 us
    reduce_scatter x1, waiting for transfers between devices, shards(): lax.psum_scatter(lax.dot_general(whole_output, column_part[0], (((0,), (0...  12.9 us
    unnamed x41, local copies, waits for them, and re-layouts  12.5 us
    all_to_all x1, blocking collectives, shards(): lax.all_to_all(d_out, 'sp', split_axis=2, concat_axis=1, tiled=True)  12.2 us
    dot_general x4, matrix products, product(): return jnp.einsum(form, left, right, preferred_element_type=jnp.float32)  7.93 us
    all_to_all x1, starting transfers between devices, shards(): lax.all_to_all(d_attn[None], 'sp', split_axis=2, concat_axis=1, tiled=True)  5.28 us
    all_to_all x1, starting transfers between devices, shards(): lax.all_to_all(tokens_first(grads[1]), 'sp', split_axis=1, concat_axis=2,...  4.33 us
  transfers between devices with their start and end apart: 6, of which 5 were waited for; matrix products, arithmetic and copies ran while one was open for 34% of the time, Pallas kernels for 0%

commit v1 on v0

--- a/solution.py
+++ b/solution.py
@@ -1,6 +1,10 @@
+import functools
+
 import jax
 import jax.numpy as jnp
 from jax import lax
+from jax.experimental import pallas as pl
+from jax.experimental.pallas import tpu as pltpu
 from jax.sharding import PartitionSpec as P
 
 
@@ -107,7 +111,7 @@
     return (query_grad, key_grad, value_grad, grads[3][None], grad_weight)
 
 
-def solution(mesh):
+def plain_solution(mesh):
     placed = (
         P("dp", None, "sp"),
         P("dp", None, "sp"),
@@ -130,3 +134,453 @@
         ),
         check_vma=False,
     )
+
+
+MESH = pl.DeviceIdType.MESH
+PAIR = 2
+LANES = 128
+
+
+def nt(left, right):
+    return lax.dot_general(
+        left, right, (((1,), (1,)), ((), ())), preferred_element_type=jnp.float32
+    )
+
+
+def nn(left, right):
+    return lax.dot_general(
+        left, right, (((1,), (0,)), ((), ())), preferred_element_type=jnp.float32
+    )
+
+
+def kernel(
+    n_sp, n_dp, n_heads, w_chunks,
+    q_hbm, k_hbm, v_hbm, o_hbm, cum_hbm, do_hbm, w_hbm,
+    dq_out, dk_out, dv_out, dcum_out, dw_out,
+    q_ref, k_ref, v_ref, o_ref, cum_ref, dof, wbuf, prob, k_t, o_t,
+    dw_own, y_send, y_recv, z_send, z_recv, dw_acc, stage, dcum_ref,
+    in_sem, out_sem,
+    x_ssem, x_rsem, c_ssem, c_rsem, f_ssem, f_rsem,
+    wz_ssem, wz_rsem, wy_ssem, wy_rsem,
+    ry_ssem, ry_rsem, rz_ssem, rz_rsem,
+    g_ssem, g_rsem, g_lsem,
+):
+    sp, dp = lax.axis_index("sp"), lax.axis_index("dp")
+    n_x, n_z = n_sp // PAIR, n_dp // PAIR
+    x, core = sp // PAIR, sp % PAIR
+    z, y = dp // PAIR, dp % PAIR
+    length, head_cols = q_ref.shape
+    head_width = head_cols // n_heads
+    tokens, width = do_hbm.shape[1:]
+    w_rows = w_hbm.shape[0]
+    col_part = width // n_sp
+    scale = head_width ** (-0.5)
+    per_pair = LANES // head_width
+    n_pairs = head_cols // LANES
+    block = min(2 * LANES, length)
+    n_blocks = length // block
+    core_peer = x * PAIR + (1 - core)
+    y_peer = z * PAIR + (1 - y)
+
+    def token_rows(owner):
+        return pl.ds(pl.multiple_of(owner * tokens, tokens), tokens)
+
+    def col_at(part):
+        return pl.ds(pl.multiple_of(part * col_part, LANES), col_part)
+
+    def remote(src, dst, ssem, rsem, **where):
+        return pltpu.make_async_remote_copy(
+            src_ref=src, dst_ref=dst, send_sem=ssem, recv_sem=rsem,
+            device_id=where, device_id_type=MESH,
+        )
+
+    own_w = pl.ds(pl.multiple_of(y * w_rows, w_rows), w_rows)
+    loads = [
+        pltpu.make_async_copy(do_hbm.at[0], dof.at[token_rows(sp)], in_sem.at[0]),
+        pltpu.make_async_copy(q_hbm.at[0], q_ref, in_sem.at[2]),
+        pltpu.make_async_copy(k_hbm.at[0], k_ref, in_sem.at[3]),
+        pltpu.make_async_copy(cum_hbm.at[0], cum_ref, in_sem.at[4]),
+        pltpu.make_async_copy(v_hbm.at[0], v_ref, in_sem.at[5]),
+        pltpu.make_async_copy(o_hbm.at[0], o_ref, in_sem.at[6]),
+    ]
+    w_load = pltpu.make_async_copy(w_hbm, wbuf.at[own_w], in_sem.at[1])
+    loads[0].start()
+
+    @pl.when(z == sp)
+    def _():
+        w_load.start()
+
+    for load in loads[1:]:
+        load.start()
+
+    barrier = pltpu.get_barrier_semaphore()
+    for off in range(1, n_sp):
+        pl.semaphore_signal(
+            barrier, inc=1, device_id={"sp": (sp + off) % n_sp, "dp": dp}, device_id_type=MESH
+        )
+    for off in range(1, n_z):
+        pl.semaphore_signal(
+            barrier, inc=1,
+            device_id={"sp": sp, "dp": ((z + off) % n_z) * PAIR + y}, device_id_type=MESH,
+        )
+    pl.semaphore_signal(barrier, inc=1, device_id={"sp": sp, "dp": y_peer}, device_id_type=MESH)
+    pl.semaphore_wait(barrier, n_sp + n_z - 1)
+
+    def x_copy(off, i, owner_x, target_x):
+        part = dof.at[token_rows(owner_x * PAIR + core), col_at((target_x * PAIR + i) % n_sp)]
+        return remote(part, part, x_ssem.at[off - 1, i], x_rsem.at[off - 1, i],
+                      sp=target_x * PAIR + core, dp=dp)
+
+    def x_out(off, i):
+        return x_copy(off, i, x, (x + off) % n_x)
+
+    def x_in(off, i):
+        return x_copy(off, i, (x + n_x - off) % n_x, x)
+
+    def core_copy(owner):
+        part = dof.at[token_rows(owner)]
+        return remote(part, part, c_ssem, c_rsem, sp=core_peer, dp=dp)
+
+    def forward_copy(off, i, owner_core):
+        owner = ((x + n_x - off) % n_x) * PAIR + owner_core
+        part = dof.at[token_rows(owner), col_at((x * PAIR + i) % n_sp)]
+        return remote(part, part, f_ssem.at[off - 1, i], f_rsem.at[off - 1, i],
+                      sp=core_peer, dp=dp)
+
+    loads[0].wait()
+    for i in range(n_sp):
+        for off in range(1, n_x):
+            x_out(off, i).start()
+    core_copy(sp).start()
+
+    def forward_step(i):
+        for off in range(1, n_x):
+            x_in(off, i).wait_recv()
+            forward_copy(off, i, core).start()
+
+    chunk_rows = w_rows // w_chunks
+
+    def w_part(owner_y, c):
+        start = pl.multiple_of(owner_y * w_rows + c * chunk_rows, chunk_rows)
+        return wbuf.at[pl.ds(start, chunk_rows)]
+
+    def wz_copy(way, c, target_z):
+        return remote(w_part(y, c), w_part(y, c), wz_ssem.at[way, c], wz_rsem.at[c],
+                      sp=sp, dp=target_z * PAIR + y)
+
+    def wy_copy(owner_y, c):
+        return remote(w_part(owner_y, c), w_part(owner_y, c), wy_ssem.at[c], wy_rsem.at[c],
+                      sp=sp, dp=y_peer)
+
+    sends_up = jnp.logical_and(z >= sp, z < n_z - 1)
+    sends_down = jnp.logical_and(z <= sp, z > 0)
+
+    def w_send(c):
+        @pl.when(sends_up)
+        def _():
+            wz_copy(0, c, z + 1).start()
+
+        @pl.when(sends_down)
+        def _():
+            wz_copy(1, c, z - 1).start()
+
+        wy_copy(y, c).start()
+
+    @pl.when(z == sp)
+    def _():
+        w_load.wait()
+        for c in range(w_chunks):
+            w_send(c)
+
+    def w_step(c):
+        @pl.when(z != sp)
+        def _():
+            wz_copy(0, c, z).wait_recv()
+            w_send(c)
+
+    lane = lax.broadcasted_iota(jnp.int32, (1, LANES), 1)
+
+    def head_mask(h):
+        return lane // head_width == h % per_pair
+
+    def pair_cols(pair):
+        return pl.ds(pair * LANES, LANES)
+
+    for load in loads[1:4]:
+        load.wait()
+    cum = cum_ref[...]
+    cum_cols = jnp.concatenate([cum] * (-(-8 // n_heads)), axis=0).T
+
+    def masked_query(h):
+        return jnp.where(head_mask(h), q_ref[:, pair_cols(h // per_pair)], 0)
+
+    def probabilities(h):
+        keys = k_ref[:, pair_cols(h // per_pair)]
+        query = masked_query(h)
+        for b in range(n_blocks):
+            lo, end = b * block, (b + 1) * block
+            scores = nt(keys[:end], query[lo:end]) * scale
+            scores = scores + cum[h:h + 1, lo:end] - cum_cols[:end, h:h + 1]
+            key_pos = lax.broadcasted_iota(jnp.int32, (end, block), 0)
+            query_pos = lo + lax.broadcasted_iota(jnp.int32, (end, block), 1)
+            scores = jnp.where(key_pos <= query_pos, scores, -1e30)
+            weights = jnp.exp(scores - jnp.max(scores, axis=0, keepdims=True))
+            weights = weights * (1.0 / jnp.sum(weights, axis=0, keepdims=True))
+            prob[h, :end, lo:end] = weights
+
+    steps = max(n_sp, w_chunks, n_heads)
+    for i in range(steps):
+        if i < n_heads:
+            probabilities(i)
+        if i == 0:
+            k_t[...] = k_ref[...].T
+        if i == 1:
+            loads[4].wait()
+            loads[5].wait()
+            o_t[...] = o_ref[...].T
+        if i < n_sp:
+            forward_step(i)
+        if i < w_chunks:
+            w_step(i)
+
+    core_copy(core_peer).wait_recv()
+    for i in range(n_sp):
+        for off in range(1, n_x):
+            forward_copy(off, i, 1 - core).wait_recv()
+    d_cols = dof[:, col_at(sp)]
+
+    def z_at(k):
+        return (z + k) % n_z
+
+    def dw_rows(k, owner_y):
+        return pl.ds(pl.multiple_of((z_at(k) * PAIR + owner_y) * w_rows, w_rows), w_rows)
+
+    def ry_copy(k):
+        return remote(y_send.at[k], y_recv.at[k], ry_ssem.at[k], ry_rsem.at[k], sp=sp, dp=y_peer)
+
+    def rz_copy(k):
+        return remote(z_send.at[k], z_recv.at[k], rz_ssem.at[k], rz_rsem.at[k],
+                      sp=sp, dp=z_at(k) * PAIR + y)
+
+    z_order = [k % n_z for k in range(1, n_z + 1)]
+    for k in z_order:
+        y_send[k] = nn(o_t[dw_rows(k, 1 - y), :], d_cols).astype(jnp.bfloat16)
+        ry_copy(k).start()
+    for k in z_order:
+        dw_own[k] = nn(o_t[dw_rows(k, y), :], d_cols)
+
+    def dw_step(k):
+        ry_copy(k).wait_recv()
+        total = dw_own[k] + y_recv[k].astype(jnp.float32)
+        if k == 0:
+            dw_acc[...] = total
+        else:
+            z_send[k] = total.astype(jnp.bfloat16)
+            rz_copy(k).start()
+
+    for c in range(w_chunks):
+        wy_copy(1 - y, c).wait_recv()
+    d_attn = nt(dof[...], wbuf[...]).astype(jnp.bfloat16)
+    outs = (dq_out, dk_out, dv_out)
+
+    def grad_copy(a, pair, off):
+        target = (sp + off) % n_sp
+        cols = pl.ds(pl.multiple_of(sp * head_cols + pair * LANES, LANES), LANES)
+        return remote(stage.at[a, token_rows(target), pair_cols(pair)],
+                      outs[a].at[0, :, cols],
+                      g_ssem.at[a, pair, off - 1], g_rsem.at[a, pair, off - 1], sp=target, dp=dp)
+
+    def grad_keep(a, pair):
+        cols = pl.ds(pl.multiple_of(sp * head_cols + pair * LANES, LANES), LANES)
+        return pltpu.make_async_copy(stage.at[a, token_rows(sp), pair_cols(pair)],
+                                     outs[a].at[0, :, cols], g_lsem.at[a, pair])
+
+    def add_rows(totals, part):
+        for b in range(part.shape[0] // block):
+            piece = part[b * block:(b + 1) * block]
+            totals[b] = piece if totals[b] is None else totals[b] + piece
+
+    def pair_gradients(pair):
+        cot = d_attn[:, pair * LANES:(pair + 1) * LANES]
+        own_out = o_ref[:, pl.ds(pl.multiple_of(sp * head_cols + pair * LANES, LANES), LANES)]
+        values = v_ref[:, pair_cols(pair)]
+        row = lax.broadcasted_iota(jnp.int32, (8, LANES), 0)
+        picks = (lax.broadcasted_iota(jnp.int32, (8, LANES), 1) // head_width == row)
+        dots = lax.dot_general(
+            picks.astype(jnp.float32), cot.astype(jnp.float32) * own_out.astype(jnp.float32),
+            (((1,), (1,)), ((), ())), precision=lax.Precision.HIGHEST,
+            preferred_element_type=jnp.float32,
+        )
+        key_total, value_total, query_total = [None] * n_blocks, [None] * n_blocks, []
+        for sub in range(per_pair):
+            h = pair * per_pair + sub
+            cot_h = jnp.where(head_mask(h), cot, 0)
+            query_h = masked_query(h)
+            keys_t = k_t[h * head_width:(h + 1) * head_width, :]
+            query_parts, row_sums, col_sums = [], [], [None] * n_blocks
+            for b in range(n_blocks):
+                lo, end = b * block, (b + 1) * block
+                weights = prob[h, :end, lo:end]
+                d_prob = nt(values[:end], cot_h[lo:end])
+                score_b = (weights * (d_prob - dots[sub:sub + 1, lo:end])).astype(jnp.bfloat16)
+                add_rows(value_total, nn(weights.astype(jnp.bfloat16), cot_h[lo:end]))
+                add_rows(key_total, nn(score_b, query_h[lo:end]))
+                query_parts.append(nn(keys_t[:, :end], score_b))
+                row_sums.append(nn(jnp.ones((8, end), jnp.bfloat16), score_b))
+                col_sum = nt(jnp.ones((8, block), jnp.bfloat16), score_b)
+                for j in range(b + 1):
+                    piece = col_sum[:, j * block:(j + 1) * block]
+                    col_sums[j] = piece if col_sums[j] is None else col_sums[j] + piece
+            d_cum = jnp.concatenate(row_sums, axis=1) - jnp.concatenate(col_sums, axis=1)
+            dcum_ref[h:h + 1, :] = d_cum[:1]
+            query_total.append(jnp.concatenate(query_parts, axis=1))
+        cols = pair_cols(pair)
+        stage[0, :, cols] = (jnp.concatenate(query_total, axis=0).T * scale).astype(jnp.bfloat16)
+        stage[1, :, cols] = (jnp.concatenate(key_total, axis=0) * scale).astype(jnp.bfloat16)
+        stage[2, :, cols] = jnp.concatenate(value_total, axis=0).astype(jnp.bfloat16)
+        for off in range(1, n_sp):
+            for a in range(3):
+                grad_copy(a, pair, off).start()
+        for a in range(3):
+            grad_keep(a, pair).start()
+
+    todo = list(z_order)
+    for pair in range(n_pairs):
+        pair_gradients(pair)
+        if todo:
+            dw_step(todo.pop(0))
+    while todo:
+        dw_step(todo.pop(0))
+
+    total = dw_acc[...]
+    for k in range(1, n_z):
+        rz_copy(k).wait_recv()
+        total = total + z_recv[k].astype(jnp.float32)
+    dw_acc[...] = total
+    results = [
+        pltpu.make_async_copy(dw_acc, dw_out, out_sem.at[0]),
+        pltpu.make_async_copy(dcum_ref, dcum_out.at[0], out_sem.at[1]),
+    ]
+    for result in results:
+        result.start()
+
+    for i in range(n_sp):
+        for off in range(1, n_x):
+            x_out(off, i).wait_send()
+            forward_copy(off, i, core).wait_send()
+    core_copy(sp).wait_send()
+    for c in range(w_chunks):
+        wy_copy(y, c).wait_send()
+
+        @pl.when(sends_up)
+        def _():
+            wz_copy(0, c, z + 1).wait_send()
+
+        @pl.when(sends_down)
+        def _():
+            wz_copy(1, c, z - 1).wait_send()
+
+    for k in range(n_z):
+        ry_copy(k).wait_send()
+        if k:
+            rz_copy(k).wait_send()
+    for pair in range(n_pairs):
+        for a in range(3):
+            for off in range(1, n_sp):
+                grad_copy(a, pair, off).wait()
+            grad_keep(a, pair).wait()
+    for result in results:
+        result.wait()
+
+
+def fits(mesh, query, cum, d_out, w_out):
+    n_sp, n_dp = mesh.shape["sp"], mesh.shape["dp"]
+    head_cols, n_heads = query.shape[2] // n_sp, cum.shape[1] // n_sp
+    length, width = d_out.shape[1], d_out.shape[2]
+    w_rows = w_out.shape[0] // n_dp
+    if head_cols % LANES or n_heads == 0 or 8 % n_heads:
+        return False
+    if LANES % (head_cols // n_heads) or length % (2 * LANES) or (width // n_sp) % LANES:
+        return False
+    if n_sp % PAIR or n_dp != PAIR * n_sp or head_cols != PAIR * w_rows or w_rows % 64:
+        return False
+    held = 4 * n_heads * length**2 + 2 * length * width + 8 * length * query.shape[2]
+    return held < 32 * 2**20
+
+
+def fused_shards(n_sp, n_dp, query, keys, values, output, cum, d_out, w_out):
+    length, head_cols = query.shape[1:]
+    attn = output.shape[2]
+    n_heads = cum.shape[1]
+    tokens, width = d_out.shape[1:]
+    w_rows = w_out.shape[0]
+    n_x, n_z, col_part = n_sp // PAIR, n_dp // PAIR, width // n_sp
+    w_chunks = 4
+    bf16, f32 = jnp.bfloat16, jnp.float32
+    dma = pltpu.SemaphoreType.DMA
+    n_pairs = head_cols // LANES
+    anywhere = pl.BlockSpec(memory_space=pl.ANY)
+    grad = jax.ShapeDtypeStruct((1, tokens, attn), bf16)
+    return pl.pallas_call(
+        functools.partial(kernel, n_sp, n_dp, n_heads, w_chunks),
+        out_shape=(
+            grad, grad, grad,
+            jax.ShapeDtypeStruct(cum.shape, f32),
+            jax.ShapeDtypeStruct((w_rows, col_part), f32),
+        ),
+        in_specs=[anywhere] * 7,
+        out_specs=[anywhere] * 5,
+        scratch_shapes=[
+            pltpu.VMEM((length, head_cols), bf16),
+            pltpu.VMEM((length, head_cols), bf16),
+            pltpu.VMEM((length, head_cols), bf16),
+            pltpu.VMEM((length, attn), bf16),
+            pltpu.VMEM(cum.shape[1:], f32),
+            pltpu.VMEM((length, width), bf16),
+            pltpu.VMEM((PAIR * w_rows, width), bf16),
+            pltpu.VMEM((n_heads, length, length), f32),
+            pltpu.VMEM((head_cols, length), bf16),
+            pltpu.VMEM((attn, length), bf16),
+            pltpu.VMEM((n_z, w_rows, col_part), f32),
+            pltpu.VMEM((n_z, w_rows, col_part), bf16),
+            pltpu.VMEM((n_z, w_rows, col_part), bf16),
+            pltpu.VMEM((n_z, w_rows, col_part), bf16),
+            pltpu.VMEM((n_z, w_rows, col_part), bf16),
+            pltpu.VMEM((w_rows, col_part), f32),
+            pltpu.VMEM((3, length, head_cols), bf16),
+            pltpu.VMEM(cum.shape[1:], f32),
+            dma((7,)), dma((2,)),
+            dma((n_x - 1, n_sp)), dma((n_x - 1, n_sp)), dma, dma,
+            dma((n_x - 1, n_sp)), dma((n_x - 1, n_sp)),
+            dma((2, w_chunks)), dma((w_chunks,)), dma((w_chunks,)), dma((w_chunks,)),
+            dma((n_z,)), dma((n_z,)), dma((n_z,)), dma((n_z,)),
+            dma((3, n_pairs, n_sp - 1)), dma((3, n_pairs, n_sp - 1)), dma((3, n_pairs)),
+        ],
+        compiler_params=pltpu.CompilerParams(
+            collective_id=0, has_side_effects=True, vmem_limit_bytes=48 * 2**20
+        ),
+    )(query, keys, values, output, cum, d_out, w_out)
+
+
+def solution(mesh):
+    n_sp, n_dp = mesh.shape["sp"], mesh.shape["dp"]
+    placed = (
+        P("dp", None, "sp"), P("dp", None, "sp"), P("dp", None, "sp"), P("dp", None, None),
+        P("dp", "sp", None), P("dp", "sp", None), P("dp", None),
+    )
+    results = (
+        P("dp", "sp", None), P("dp", "sp", None), P("dp", "sp", None), P("dp", "sp", None),
+        P("dp", "sp"),
+    )
+
+    def run(query, keys, values, output, cum, d_out, w_out):
+        if fits(mesh, query, cum, d_out, w_out):
+            body = functools.partial(fused_shards, n_sp, n_dp)
+            step = jax.shard_map(
+                body, mesh=mesh, in_specs=placed, out_specs=results, check_vma=False
+            )
+        else:
+            step = plain_solution(mesh)
+        return step(query, keys, values, output, cum, d_out, w_out)
+
+    return run

time: 164 us -> 55.2 us (0.34); the launches traced: 161 us -> 54.8 us
  waiting for transfers between devices: 62.7 us -> 0 us
  Pallas kernels: 0 us -> 43.9 us
  other arithmetic: 21.9 us -> 0 us
  starting transfers between devices: 17.4 us -> 0 us
  matrix products: 17.1 us -> 0 us
  between operations: 14.4 us -> 0.66 us
  blocking collectives: 12.2 us -> 0 us
  local copies, waits for them, and re-layouts: 15.4 us -> 10.3 us
    all_gather x1 -> x0, waiting for transfers between devices: 44.6 us -> none  [shards(): lax.all_gather(w_out, 'dp', axis=0, tiled=True)]
    pallas_call x0 -> x1, Pallas kernels: none -> 43.9 us  [fused_shards(): pl.pallas_call(functools.partial(kernel, n_sp, n_dp, n_heads, w_chunks),...]
    unnamed x5 -> x0, other arithmetic: 21.1 us -> none
    all_to_all x4 -> x0, starting transfers between devices: 17.4 us -> none  [the longest x1 5.28 us: shards(): lax.all_to_all(d_attn[None], 'sp', split_axis=2, concat_axis=1, tiled=True)]
    dot_general x6 -> x0, matrix products: 13.7 us -> none  [the longest x4 7.93 us: product(): return jnp.einsum(form, left, right, preferred_element_type=jnp.float32)]
    reduce_scatter x1 -> x0, waiting for transfers between devices: 12.9 us -> none  [shards(): lax.psum_scatter(lax.dot_general(whole_output, column_part[0], (((0,), (0...]
    all_to_all x1 -> x0, blocking collectives: 12.2 us -> none  [shards(): lax.all_to_all(d_out, 'sp', split_axis=2, concat_axis=1, tiled=True)]
    all_to_all x4 -> x0, waiting for transfers between devices: 4.53 us -> none  [the longest x1 1.74 us: shards(): lax.all_to_all(tokens_first(grads[2]), 'sp', split_axis=1, concat_axis=2,...]
  transfers between devices with their start and end apart: 6 -> 0, of which waited for: 5 -> 0; matrix products, arithmetic and copies ran while one was open for 34% -> 0% of each run, Pallas kernels for 0% -> 0%
where the time goes in v1:
time: 55.2 us; the launch traced here: 54.8 us
  Pallas kernels  43.9 us (80%)
  local copies, waits for them, and re-layouts  10.3 us (19%)
  between operations  0.66 us (1%)
    pallas_call x1, Pallas kernels, fused_shards(): pl.pallas_call(functools.partial(kernel, n_sp, n_dp, n_heads, w_chunks),...  43.9 us
    unnamed x19, local copies, waits for them, and re-layouts  10.3 us

profile of v1, /device:TPU:1, one launch (start us, length us, event | category | flops | bytes accessed | tf_op | source)
XLA Modules:
  0.0 54.8 jit_solution(17712004823401326660)
XLA Ops:
  0.6 0.0 copy-start
  0.6 1.2 %copy-done = bf16[1,512,1024]{2,1,0:T(8,128)(2,1)S(1)} copy-done((bf16[1,512,1024]{2,1,0:T(8,128)(2,1)S(1)}, bf16[1,512,1024]{2,1,0:T(8,128)(2,1)}, u32[]{:S(2)}) %copy-start) | copy-done | bytes 1048600
  1.9 0.0 copy-start.1
  1.9 1.0 %copy-done.1 = bf16[1,128,2048]{2,1,0:T(8,128)(2,1)S(1)} copy-done((bf16[1,128,2048]{2,1,0:T(8,128)(2,1)S(1)}, bf16[1,128,2048]{2,1,0:T(8,128)(2,1)}, u32[]{:S(2)}) %copy-start.1) | copy-done | bytes 524312
  2.9 0.0 copy-start.2
  2.9 1.0 %copy-done.2 = bf16[128,2048]{1,0:T(8,128)(2,1)S(1)} copy-done((bf16[128,2048]{1,0:T(8,128)(2,1)S(1)}, bf16[128,2048]{1,0:T(8,128)(2,1)}, u32[]{:S(2)}) %copy-start.2) | copy-done | bytes 524312
  3.9 0.0 copy-start.3
  3.9 0.9 %copy-done.3 = bf16[1,512,256]{2,1,0:T(8,128)(2,1)S(1)} copy-done((bf16[1,512,256]{2,1,0:T(8,128)(2,1)S(1)}, bf16[1,512,256]{2,1,0:T(8,128)(2,1)}, u32[]{:S(2)}) %copy-start.3) | copy-done | bytes 262168
  4.9 0.0 copy-start.4
  4.9 0.9 %copy-done.4 = bf16[1,512,256]{2,1,0:T(8,128)(2,1)S(1)} copy-done((bf16[1,512,256]{2,1,0:T(8,128)(2,1)S(1)}, bf16[1,512,256]{2,1,0:T(8,128)(2,1)}, u32[]{:S(2)}) %copy-start.4) | copy-done | bytes 262168
  5.8 0.0 copy-start.5
  5.8 0.9 %copy-done.5 = bf16[1,512,256]{2,1,0:T(8,128)(2,1)S(1)} copy-done((bf16[1,512,256]{2,1,0:T(8,128)(2,1)S(1)}, bf16[1,512,256]{2,1,0:T(8,128)(2,1)}, u32[]{:S(2)}) %copy-start.5) | copy-done | bytes 262168
  6.8 0.0 copy-start.6
  6.8 0.7 %copy-done.6 = f32[1,4,512]{2,1,0:T(4,128)S(1)} copy-done((f32[1,4,512]{2,1,0:T(4,128)S(1)}, f32[1,4,512]{2,1,0:T(4,128)}, u32[]{:S(2)}) %copy-start.6) | copy-done | bytes 8216
  7.5 43.9 %shard_map.110 = (bf16[1,128,1024]{2,1,0:T(8,128)(2,1)S(1)}, bf16[1,128,1024]{2,1,0:T(8,128)(2,1)S(1)}, bf16[1,128,1024]{2,1,0:T(8,128)(2,1)S(1)}, f32[1,4,512]{2,1,0:T(4,128)S(1)}, f32[128,512]{1,0:T(8,128)S(1)}) custom-call(bf16[1,512,256]{2,1,0:T(8,128)(2,1)S(1)} %copy-done.3, bf16[1,512,256]{2,1,0:T(8,128)(2,1)S(1)} %copy-done.4, ...), custom_call_target="tpu_custom_call" | custom-call | tf_op jit(solution)/shard_map/pallas_call | solution.py:524
  51.4 0.7 %copy.17 = bf16[1,128,1024]{2,1,0:T(8,128)(2,1)} copy(bf16[1,128,1024]{2,1,0:T(8,128)(2,1)S(1)} %get-tuple-element.10) | data formatting | bytes 524288
  52.1 0.7 %copy.18 = bf16[1,128,1024]{2,1,0:T(8,128)(2,1)} copy(bf16[1,128,1024]{2,1,0:T(8,128)(2,1)S(1)} %get-tuple-element.11) | data formatting | bytes 524288
  52.8 0.7 %copy.19 = bf16[1,128,1024]{2,1,0:T(8,128)(2,1)} copy(bf16[1,128,1024]{2,1,0:T(8,128)(2,1)S(1)} %get-tuple-element.12) | data formatting | bytes 524288
  53.5 0.6 %copy.20 = f32[1,4,512]{2,1,0:T(4,128)} copy(f32[1,4,512]{2,1,0:T(4,128)S(1)} %get-tuple-element.13) | data formatting | bytes 16384
  54.1 0.7 %copy.21 = f32[128,512]{1,0:T(8,128)} copy(f32[128,512]{1,0:T(8,128)S(1)} %get-tuple-element.14) | data formatting | bytes 524288
Async XLA Ops:
  0.6 1.2 %copy-start = (bf16[1,512,1024]{2,1,0:T(8,128)(2,1)S(1)}, bf16[1,512,1024]{2,1,0:T(8,128)(2,1)}, u32[]{:S(2)}) copy-start(bf16[1,512,1024]{2,1,0:T(8,128)(2,1)} %o_hbm.1) | copy-start | bytes 3145732
  1.9 1.0 %copy-start.1 = (bf16[1,128,2048]{2,1,0:T(8,128)(2,1)S(1)}, bf16[1,128,2048]{2,1,0:T(8,128)(2,1)}, u32[]{:S(2)}) copy-start(bf16[1,128,2048]{2,1,0:T(8,128)(2,1)} %do_hbm.1) | copy-start | bytes 1572868
  2.9 1.0 %copy-start.2 = (bf16[128,2048]{1,0:T(8,128)(2,1)S(1)}, bf16[128,2048]{1,0:T(8,128)(2,1)}, u32[]{:S(2)}) copy-start(bf16[128,2048]{1,0:T(8,128)(2,1)} %w_hbm.1) | copy-start | bytes 1572868
  3.9 0.9 %copy-start.3 = (bf16[1,512,256]{2,1,0:T(8,128)(2,1)S(1)}, bf16[1,512,256]{2,1,0:T(8,128)(2,1)}, u32[]{:S(2)}) copy-start(bf16[1,512,256]{2,1,0:T(8,128)(2,1)} %q_hbm.1) | copy-start | bytes 786436
  4.9 0.9 %copy-start.4 = (bf16[1,512,256]{2,1,0:T(8,128)(2,1)S(1)}, bf16[1,512,256]{2,1,0:T(8,128)(2,1)}, u32[]{:S(2)}) copy-start(bf16[1,512,256]{2,1,0:T(8,128)(2,1)} %k_hbm.1) | copy-start | bytes 786436
  5.8 0.9 %copy-start.5 = (bf16[1,512,256]{2,1,0:T(8,128)(2,1)S(1)}, bf16[1,512,256]{2,1,0:T(8,128)(2,1)}, u32[]{:S(2)}) copy-start(bf16[1,512,256]{2,1,0:T(8,128)(2,1)} %v_hbm.1) | copy-start | bytes 786436
  6.8 0.7 %copy-start.6 = (f32[1,4,512]{2,1,0:T(4,128)S(1)}, f32[1,4,512]{2,1,0:T(4,128)}, u32[]{:S(2)}) copy-start(f32[1,4,512]{2,1,0:T(4,128)} %cum_hbm.1) | copy-start | bytes 24580

commit v2 on v1

--- a/solution.py
+++ b/solution.py
@@ -493,6 +493,17 @@
         result.wait()
 
 
+def hand_over(*refs):
+    count = len(refs) // 2
+    copies = [
+        pltpu.make_async_copy(refs[i], refs[count + i], refs[-1].at[i]) for i in range(count)
+    ]
+    for copy in copies:
+        copy.start()
+    for copy in copies:
+        copy.wait()
+
+
 def fits(mesh, query, cum, d_out, w_out):
     n_sp, n_dp = mesh.shape["sp"], mesh.shape["dp"]
     head_cols, n_heads = query.shape[2] // n_sp, cum.shape[1] // n_sp
@@ -509,6 +520,7 @@
 
 
 def fused_shards(n_sp, n_dp, query, keys, values, output, cum, d_out, w_out):
+    arrays = (query, keys, values, output, cum, d_out, w_out)
     length, head_cols = query.shape[1:]
     attn = output.shape[2]
     n_heads = cum.shape[1]
@@ -520,15 +532,16 @@
     dma = pltpu.SemaphoreType.DMA
     n_pairs = head_cols // LANES
     anywhere = pl.BlockSpec(memory_space=pl.ANY)
+    from_hbm = pl.BlockSpec(memory_space=pltpu.HBM)
     grad = jax.ShapeDtypeStruct((1, tokens, attn), bf16)
-    return pl.pallas_call(
+    found = pl.pallas_call(
         functools.partial(kernel, n_sp, n_dp, n_heads, w_chunks),
         out_shape=(
             grad, grad, grad,
             jax.ShapeDtypeStruct(cum.shape, f32),
             jax.ShapeDtypeStruct((w_rows, col_part), f32),
         ),
-        in_specs=[anywhere] * 7,
+        in_specs=[from_hbm] * 7,
         out_specs=[anywhere] * 5,
         scratch_shapes=[
             pltpu.VMEM((length, head_cols), bf16),
@@ -559,7 +572,15 @@
         compiler_params=pltpu.CompilerParams(
             collective_id=0, has_side_effects=True, vmem_limit_bytes=48 * 2**20
         ),
-    )(query, keys, values, output, cum, d_out, w_out)
+    )(*[pltpu.with_memory_space_constraint(array, pltpu.HBM) for array in arrays])
+    return pl.pallas_call(
+        hand_over,
+        out_shape=[jax.ShapeDtypeStruct(part.shape, part.dtype) for part in found],
+        in_specs=[anywhere] * len(found),
+        out_specs=[from_hbm] * len(found),
+        scratch_shapes=[dma((len(found),))],
+        compiler_params=pltpu.CompilerParams(vmem_limit_bytes=2**20),
+    )(*found)
 
 
 def solution(mesh):

time: 55.2 us -> 45.5 us (0.82)
  local copies, waits for them, and re-layouts: 10.3 us -> 0 us
  Pallas kernels: 43.9 us -> 44.7 us
    unnamed x19 -> x0, local copies, waits for them, and re-layouts: 10.3 us -> none
    pallas_call x0 -> x1, Pallas kernels: none -> 1.01 us  [fused_shards(): pl.pallas_call(hand_over, out_shape=[jax.ShapeDtypeStruct(part.shape, par...]
where the time goes in v2:
time: 45.5 us; the launch traced here: 45.4 us
  Pallas kernels  44.7 us (98%)
  between operations  0.64 us (1%)
    pallas_call x1, Pallas kernels, fused_shards(): pl.pallas_call(functools.partial(kernel, n_sp, n_dp, n_heads, w_chunks),...  43.7 us
    pallas_call x1, Pallas kernels, fused_shards(): pl.pallas_call(hand_over, out_shape=[jax.ShapeDtypeStruct(part.shape, par...  1.01 us

profile of v2, /device:TPU:1, one launch (start us, length us, event | category | flops | bytes accessed | tf_op | source)
XLA Modules:
  0.0 45.4 jit_solution(6735644813225589803)
XLA Ops:
  0.6 43.7 %shard_map.110 = (bf16[1,128,1024]{2,1,0:T(8,128)(2,1)S(1)}, bf16[1,128,1024]{2,1,0:T(8,128)(2,1)S(1)}, bf16[1,128,1024]{2,1,0:T(8,128)(2,1)S(1)}, f32[1,4,512]{2,1,0:T(4,128)S(1)}, f32[128,512]{1,0:T(8,128)S(1)}) custom-call(bf16[1,512,256]{2,1,0:T(8,128)(2,1)} %q_hbm.1, bf16[1,512,256]{2,1,0:T(8,128)(2,1)} %k_hbm.1, bf16[1,512,256]{2,1,0:T(8,128)(2,1)} %v_hbm.1, ...), custom_call_target="tpu_custom_call" | custom-call | tf_op jit(solution)/shard_map/pallas_call | solution.py:537
  44.4 1.0 %shard_map.111 = (bf16[1,128,1024]{2,1,0:T(8,128)(2,1)}, bf16[1,128,1024]{2,1,0:T(8,128)(2,1)}, bf16[1,128,1024]{2,1,0:T(8,128)(2,1)}, f32[1,4,512]{2,1,0:T(4,128)}, f32[128,512]{1,0:T(8,128)}) custom-call(bf16[1,128,1024]{2,1,0:T(8,128)(2,1)S(1)} %get-tuple-element.10.refs_0_, bf16[1,128,1024]{2,1,0:T(8,128)(2,1)S(1)} %get-tuple-element.11.refs_1_, ...), custom_call_target="tpu_custom_call" | custom-call | tf_op jit(solution)/shard_map/pallas_call | solution.py:576

commit v3 on v2

--- a/solution.py
+++ b/solution.py
@@ -300,23 +300,23 @@
 
     lane = lax.broadcasted_iota(jnp.int32, (1, LANES), 1)
 
-    def head_mask(h):
-        return lane // head_width == h % per_pair
+    def head_mask(sub):
+        return lane // head_width == sub
 
     def pair_cols(pair):
-        return pl.ds(pair * LANES, LANES)
+        return pl.ds(pl.multiple_of(pair * LANES, LANES), LANES)
 
     for load in loads[1:4]:
         load.wait()
     cum = cum_ref[...]
     cum_cols = jnp.concatenate([cum] * (-(-8 // n_heads)), axis=0).T
 
-    def masked_query(h):
-        return jnp.where(head_mask(h), q_ref[:, pair_cols(h // per_pair)], 0)
+    def masked_query(pair, sub):
+        return jnp.where(head_mask(sub), q_ref[:, pair_cols(pair)], 0)
 
     def probabilities(h):
         keys = k_ref[:, pair_cols(h // per_pair)]
-        query = masked_query(h)
+        query = masked_query(h // per_pair, h % per_pair)
         for b in range(n_blocks):
             lo, end = b * block, (b + 1) * block
             scores = nt(keys[:end], query[lo:end]) * scale
@@ -328,29 +328,17 @@
             weights = weights * (1.0 / jnp.sum(weights, axis=0, keepdims=True))
             prob[h, :end, lo:end] = weights
 
-    steps = max(n_sp, w_chunks, n_heads)
-    for i in range(steps):
-        if i < n_heads:
-            probabilities(i)
-        if i == 0:
-            k_t[...] = k_ref[...].T
-        if i == 1:
-            loads[4].wait()
-            loads[5].wait()
-            o_t[...] = o_ref[...].T
-        if i < n_sp:
-            forward_step(i)
-        if i < w_chunks:
-            w_step(i)
-
-    core_copy(core_peer).wait_recv()
-    for i in range(n_sp):
-        for off in range(1, n_x):
-            forward_copy(off, i, 1 - core).wait_recv()
-    d_cols = dof[:, col_at(sp)]
+    def key_transpose():
+        k_t[...] = k_ref[...].T
+
+    def output_transpose():
+        loads[4].wait()
+        loads[5].wait()
+        o_t[...] = o_ref[...].T
 
     def z_at(k):
-        return (z + k) % n_z
+        bits = [(b, (z // b) % 2) for b in (2**i for i in range(n_z.bit_length() - 1))]
+        return sum(b * (1 - bit if k & b else bit) for b, bit in bits)
 
     def dw_rows(k, owner_y):
         return pl.ds(pl.multiple_of((z_at(k) * PAIR + owner_y) * w_rows, w_rows), w_rows)
@@ -362,14 +350,31 @@
         return remote(z_send.at[k], z_recv.at[k], rz_ssem.at[k], rz_rsem.at[k],
                       sp=sp, dp=z_at(k) * PAIR + y)
 
-    z_order = [k % n_z for k in range(1, n_z + 1)]
-    for k in z_order:
-        y_send[k] = nn(o_t[dw_rows(k, 1 - y), :], d_cols).astype(jnp.bfloat16)
-        ry_copy(k).start()
-    for k in z_order:
-        dw_own[k] = nn(o_t[dw_rows(k, y), :], d_cols)
-
-    def dw_step(k):
+    half = n_z // 2
+    z_order = list(range(half, n_z)) + list(range(half - 1, -1, -1))
+    def columns_arrive(first, last):
+        for i in range(first, last):
+            for off in range(1, n_x):
+                forward_copy(off, i, 1 - core).wait_recv()
+
+    def columns_ready():
+        core_copy(core_peer).wait_recv()
+        columns_arrive(0, PAIR)
+
+    def dw_away(n):
+        k = z_order[n]
+        product = nn(o_t[dw_rows(k, 1 - y), :], dof[:, col_at(sp)])
+        y_send[k] = product.astype(jnp.bfloat16)
+
+    def dw_keep(n):
+        k = z_order[n]
+        dw_own[k] = nn(o_t[dw_rows(k, y), :], dof[:, col_at(sp)])
+
+    def dw_exchange(n):
+        ry_copy(z_order[n]).start()
+
+    def dw_step(n):
+        k = z_order[n]
         ry_copy(k).wait_recv()
         total = dw_own[k] + y_recv[k].astype(jnp.float32)
         if k == 0:
@@ -378,31 +383,39 @@
             z_send[k] = total.astype(jnp.bfloat16)
             rz_copy(k).start()
 
-    for c in range(w_chunks):
-        wy_copy(1 - y, c).wait_recv()
-    d_attn = nt(dof[...], wbuf[...]).astype(jnp.bfloat16)
     outs = (dq_out, dk_out, dv_out)
 
-    def grad_copy(a, pair, off):
+    def grad_cols(pair):
+        return pl.ds(pl.multiple_of(sp * head_cols + pair * LANES, LANES), LANES)
+
+    def pair_of(turn):
+        return y if turn == 0 else 1 - y
+
+    def grad_copy(a, turn, off):
         target = (sp + off) % n_sp
-        cols = pl.ds(pl.multiple_of(sp * head_cols + pair * LANES, LANES), LANES)
+        pair = pair_of(turn)
         return remote(stage.at[a, token_rows(target), pair_cols(pair)],
-                      outs[a].at[0, :, cols],
-                      g_ssem.at[a, pair, off - 1], g_rsem.at[a, pair, off - 1], sp=target, dp=dp)
-
-    def grad_keep(a, pair):
-        cols = pl.ds(pl.multiple_of(sp * head_cols + pair * LANES, LANES), LANES)
+                      outs[a].at[0, :, grad_cols(pair)],
+                      g_ssem.at[a, turn, off - 1], g_rsem.at[a, turn, off - 1], sp=target, dp=dp)
+
+    def grad_keep(a, turn):
+        pair = pair_of(turn)
         return pltpu.make_async_copy(stage.at[a, token_rows(sp), pair_cols(pair)],
-                                     outs[a].at[0, :, cols], g_lsem.at[a, pair])
+                                     outs[a].at[0, :, grad_cols(pair)], g_lsem.at[a, turn])
 
     def add_rows(totals, part):
         for b in range(part.shape[0] // block):
             piece = part[b * block:(b + 1) * block]
             totals[b] = piece if totals[b] is None else totals[b] + piece
 
-    def pair_gradients(pair):
-        cot = d_attn[:, pair * LANES:(pair + 1) * LANES]
-        own_out = o_ref[:, pl.ds(pl.multiple_of(sp * head_cols + pair * LANES, LANES), LANES)]
+    def pair_gradients(turn):
+        pair = pair_of(turn)
+        if turn:
+            for c in range(w_chunks):
+                wy_copy(1 - y, c).wait_recv()
+        pair_w = wbuf[pl.ds(pl.multiple_of(pair * w_rows, w_rows), w_rows), :]
+        cot = nt(dof[...], pair_w).astype(jnp.bfloat16)
+        own_out = o_ref[:, grad_cols(pair)]
         values = v_ref[:, pair_cols(pair)]
         row = lax.broadcasted_iota(jnp.int32, (8, LANES), 0)
         picks = (lax.broadcasted_iota(jnp.int32, (8, LANES), 1) // head_width == row)
@@ -414,9 +427,9 @@
         key_total, value_total, query_total = [None] * n_blocks, [None] * n_blocks, []
         for sub in range(per_pair):
             h = pair * per_pair + sub
-            cot_h = jnp.where(head_mask(h), cot, 0)
-            query_h = masked_query(h)
-            keys_t = k_t[h * head_width:(h + 1) * head_width, :]
+            cot_h = jnp.where(head_mask(sub), cot, 0)
+            query_h = masked_query(pair, sub)
+            keys_t = k_t[pl.ds(pl.multiple_of(h * head_width, head_width), head_width), :]
             query_parts, row_sums, col_sums = [], [], [None] * n_blocks
             for b in range(n_blocks):
                 lo, end = b * block, (b + 1) * block
@@ -432,7 +445,7 @@
                     piece = col_sum[:, j * block:(j + 1) * block]
                     col_sums[j] = piece if col_sums[j] is None else col_sums[j] + piece
             d_cum = jnp.concatenate(row_sums, axis=1) - jnp.concatenate(col_sums, axis=1)
-            dcum_ref[h:h + 1, :] = d_cum[:1]
+            dcum_ref[pl.ds(h, 1), :] = d_cum[:1]
             query_total.append(jnp.concatenate(query_parts, axis=1))
         cols = pair_cols(pair)
         stage[0, :, cols] = (jnp.concatenate(query_total, axis=0).T * scale).astype(jnp.bfloat16)
@@ -440,17 +453,36 @@
         stage[2, :, cols] = jnp.concatenate(value_total, axis=0).astype(jnp.bfloat16)
         for off in range(1, n_sp):
             for a in range(3):
-                grad_copy(a, pair, off).start()
+                grad_copy(a, turn, off).start()
         for a in range(3):
-            grad_keep(a, pair).start()
-
-    todo = list(z_order)
-    for pair in range(n_pairs):
-        pair_gradients(pair)
-        if todo:
-            dw_step(todo.pop(0))
-    while todo:
-        dw_step(todo.pop(0))
+            grad_keep(a, turn).start()
+
+    output_transpose()
+    key_transpose()
+    for h in range(n_heads):
+        probabilities(h)
+    sent = 0
+    for i in range(n_sp):
+        upto = min(w_chunks * (i + 1) // n_sp + 1, w_chunks)
+        for c in range(sent, upto):
+            w_step(c)
+        sent = upto
+        forward_step(i)
+    columns_ready()
+    for n in range(half):
+        dw_away(n)
+        dw_exchange(n)
+    columns_arrive(PAIR, n_sp)
+    pair_gradients(0)
+    for n in range(half, n_z):
+        dw_away(n)
+        dw_exchange(n)
+    for n in range(n_z):
+        dw_keep(n)
+    dw_step(0)
+    pair_gradients(1)
+    for n in range(1, n_z):
+        dw_step(n)
 
     total = dw_acc[...]
     for k in range(1, n_z):
@@ -484,11 +516,11 @@
         ry_copy(k).wait_send()
         if k:
             rz_copy(k).wait_send()
-    for pair in range(n_pairs):
+    for turn in range(n_pairs):
         for a in range(3):
             for off in range(1, n_sp):
-                grad_copy(a, pair, off).wait()
-            grad_keep(a, pair).wait()
+                grad_copy(a, turn, off).wait()
+            grad_keep(a, turn).wait()
     for result in results:
         result.wait()
 
@@ -513,7 +545,7 @@
         return False
     if LANES % (head_cols // n_heads) or length % (2 * LANES) or (width // n_sp) % LANES:
         return False
-    if n_sp % PAIR or n_dp != PAIR * n_sp or head_cols != PAIR * w_rows or w_rows % 64:
+    if n_sp & (n_sp - 1) or n_sp < PAIR or n_dp != PAIR * n_sp or head_cols != PAIR * LANES or w_rows != LANES:
         return False
     held = 4 * n_heads * length**2 + 2 * length * width + 8 * length * query.shape[2]
     return held < 32 * 2**20
@@ -527,7 +559,7 @@
     tokens, width = d_out.shape[1:]
     w_rows = w_out.shape[0]
     n_x, n_z, col_part = n_sp // PAIR, n_dp // PAIR, width // n_sp
-    w_chunks = 4
+    w_chunks = 8
     bf16, f32 = jnp.bfloat16, jnp.float32
     dma = pltpu.SemaphoreType.DMA
     n_pairs = head_cols // LANES

time: 45.5 us -> 41.8 us (0.919)
  the two profiles are of different devices: /device:TPU:1 before, /device:TPU:0 now
where the time goes in v3:
time: 41.8 us; the launch traced here: 41.7 us
  Pallas kernels  41 us (98%)
  between operations  0.64 us (2%)
    pallas_call x1, Pallas kernels, fused_shards(): pl.pallas_call(functools.partial(kernel, n_sp, n_dp, n_heads, w_chunks),...  40 us
    pallas_call x1, Pallas kernels, fused_shards(): pl.pallas_call(hand_over, out_shape=[jax.ShapeDtypeStruct(part.shape, par...  1.01 us

profile of v3, /device:TPU:0, one launch (start us, length us, event | category | flops | bytes accessed | tf_op | source)
XLA Modules:
  0.0 41.7 jit_solution(5641374211054466230)
XLA Ops:
  0.6 40.0 %shard_map.110 = (bf16[1,128,1024]{2,1,0:T(8,128)(2,1)S(1)}, bf16[1,128,1024]{2,1,0:T(8,128)(2,1)S(1)}, bf16[1,128,1024]{2,1,0:T(8,128)(2,1)S(1)}, f32[1,4,512]{2,1,0:T(4,128)S(1)}, f32[128,512]{1,0:T(8,128)S(1)}) custom-call(bf16[1,512,256]{2,1,0:T(8,128)(2,1)} %q_hbm.1, bf16[1,512,256]{2,1,0:T(8,128)(2,1)} %k_hbm.1, bf16[1,512,256]{2,1,0:T(8,128)(2,1)} %v_hbm.1, ...), custom_call_target="tpu_custom_call" | custom-call | tf_op jit(solution)/shard_map/pallas_call | solution.py:569
  40.7 1.0 %shard_map.111 = (bf16[1,128,1024]{2,1,0:T(8,128)(2,1)}, bf16[1,128,1024]{2,1,0:T(8,128)(2,1)}, bf16[1,128,1024]{2,1,0:T(8,128)(2,1)}, f32[1,4,512]{2,1,0:T(4,128)}, f32[128,512]{1,0:T(8,128)}) custom-call(bf16[1,128,1024]{2,1,0:T(8,128)(2,1)S(1)} %get-tuple-element.10.refs_0_, bf16[1,128,1024]{2,1,0:T(8,128)(2,1)S(1)} %get-tuple-element.11.refs_1_, ...), custom_call_target="tpu_custom_call" | custom-call | tf_op jit(solution)/shard_map/pallas_call | solution.py:608
